TPU v7x, 32 devices: a whole 2x2x4 slice. The times are simulated.
32 devices in a mesh: dp: 4 (over y, x), kv: 4 (over z), tp: 2 (over core).
Axes of the slice: x: 2, y: 2, z: 4, core: 2. Of those that a mesh axis runs over, the one named last changes fastest.
Arguments:
- tokens: bfloat16 [4, 1024, 1024], P('dp', 'kv', 'tp'), may hold values from -6 to 6
- norm_gain: float32 [1024], replicated, may hold values from 0.1 to 1.9
- w_query: bfloat16 [1024, 1024], P(None, 'tp'), may hold values from -0.1875 to 0.1875
- w_key: bfloat16 [1024, 256], P(None, 'tp'), may hold values from -0.1875 to 0.1875
- w_value: bfloat16 [1024, 256], P(None, 'tp'), may hold values from -0.1875 to 0.1875
- q_gain: float32 [64], replicated, may hold values from 0.1 to 1.9
- k_gain: float32 [64], replicated, may hold values from 0.1 to 1.9
- w_out: bfloat16 [1024, 1024], P('tp'), may hold values from -4 to 4
- chosen: int32 [4, 32, 16], P('dp', 'kv'), may hold values from -1 to 31, as said below
Outputs:
- mixed: bfloat16 [4, 1024, 1024], P('dp', 'kv', 'tp')
- log_total: float32 [4, 16, 1024], P('dp', 'tp', 'kv')
Inputs may be any that keep to these rules, and one draw needn't show every extreme that they name: Each row of chosen (one query block b) holds distinct key block numbers, all at most b, and -1 for empty entries; b itself is always present; a row is full (16 blocks) whenever at least 16 blocks may be chosen by it. Over the 8 rows of one index of kv, the chosen blocks that lie on any one other index of kv are at most 4 distinct ones, and exactly 4 of those on the index just before, for every index but the first. Some blocks are chosen far more often than others.
All inputs are finite; a program needn't handle non-finite values.
Results may differ from a plain program's by a relative error of at most 0.015.
Values may be sent and summed in bfloat16 or wider, within the bound.
A program may use at most 64 MiB of HBM per device.

v0:
```python
import math
import jax
import jax.numpy as jnp
from jax import lax
from jax.sharding import PartitionSpec as P

H = 16
HD = 64
BLK = 32
epsilon = 1e-06
alibi_reach = 4.0
masked = -1e30


def rms_norm(values, gain):
    return (
        values
        * lax.rsqrt(jnp.mean(values * values, axis=-1, keepdims=True) + epsilon)
        * gain.astype(jnp.float32)
    )


def shards(tokens, norm_gain, w_query, w_key, w_value, q_gain, k_gain, w_out, chosen):
    gathered = lax.all_gather(tokens, "tp", axis=2, tiled=True)
    seq_dev, tok_dev, model_width = gathered.shape
    n_kv = lax.axis_size("kv")
    n_tp = lax.axis_size("tp")
    kv_index = lax.axis_index("kv")
    tp_index = lax.axis_index("tp")
    heads_here = w_query.shape[1] // HD
    kv_here = w_key.shape[1] // HD
    group_size = heads_here // kv_here
    blocks_here = tok_dev // BLK
    seq_len = tok_dev * n_kv
    hidden = (
        rms_norm(gathered.astype(jnp.float32), norm_gain)
        .astype(jnp.bfloat16)
        .reshape(seq_dev * tok_dev, model_width)
    )
    queries = rms_norm(
        jnp.dot(hidden, w_query, preferred_element_type=jnp.float32).reshape(
            seq_dev, tok_dev, heads_here, HD
        ),
        q_gain,
    ).astype(jnp.bfloat16)
    key_rows = rms_norm(
        jnp.dot(hidden, w_key, preferred_element_type=jnp.float32).reshape(
            seq_dev, tok_dev, kv_here, HD
        ),
        k_gain,
    ).astype(jnp.bfloat16)
    value_rows = (
        jnp.dot(hidden, w_value, preferred_element_type=jnp.float32)
        .astype(jnp.bfloat16)
        .reshape(seq_dev, tok_dev, kv_here, HD)
    )
    queries = queries.reshape(seq_dev, blocks_here, BLK, kv_here, group_size, HD)
    head_ids = tp_index * heads_here + jnp.arange(heads_here, dtype=jnp.int32)
    slopes = jnp.exp2(-8.0 * (head_ids + 1).astype(jnp.float32) / H).reshape(kv_here, group_size)
    query_pos = (kv_index * tok_dev + jnp.arange(tok_dev, dtype=jnp.int32)).reshape(
        blocks_here, BLK
    )
    score_scale = HD ** (-0.5)

    def absorb(state_now, span_keys, span_values, key_pos, usable):
        row_max, row_sum, weighted = state_now
        key_block = key_pos // BLK
        member = jnp.any(chosen[:, :, :, None] == key_block[:, None, None, :], axis=2)
        offset = query_pos[None, :, :, None] - key_pos[:, None, None, :]
        allowed = member[:, :, None, :] & usable[:, None, None, :] & (offset >= 0)
        scores = (
            jnp.einsum(
                "sbqkgd,snkd->skgbqn", queries, span_keys, preferred_element_type=jnp.float32
            )
            * score_scale
        )
        penalty = (
            slopes[None, :, :, None, None, None]
            * offset.astype(jnp.float32)[:, None, None]
            * alibi_reach
            / seq_len
        )
        scores = jnp.where(allowed[:, None, None], scores - penalty, masked)
        new_max = jnp.maximum(row_max, jnp.max(scores, axis=-1))
        weights = jnp.where(allowed[:, None, None], jnp.exp(scores - new_max[..., None]), 0.0)
        shrink = jnp.exp(row_max - new_max)
        row_sum = row_sum * shrink + jnp.sum(weights, axis=-1)
        weighted = weighted * shrink[..., None] + jnp.einsum(
            "skgbqn,snkd->skgbqd",
            weights.astype(jnp.bfloat16),
            span_values,
            preferred_element_type=jnp.float32,
        )
        return (new_max, row_sum, weighted)

    stat_shape = (seq_dev, kv_here, group_size, blocks_here, BLK)
    initial = (
        jnp.full(stat_shape, masked, jnp.float32),
        jnp.zeros(stat_shape, jnp.float32),
        jnp.zeros(stat_shape + (HD,), jnp.float32),
    )

    def fold_piece(state_now, shard_piece, first_row):
        piece_keys, piece_values = shard_piece
        row_count = piece_keys.shape[1]
        span_len = math.gcd(row_count, tok_dev)

        def one_span(step_index, running):
            first_key = step_index * span_len
            span_keys = lax.dynamic_slice_in_dim(piece_keys, first_key, span_len, 1)
            span_values = lax.dynamic_slice_in_dim(piece_values, first_key, span_len, 1)
            key_pos = jnp.broadcast_to(
                first_row.astype(jnp.int32) + first_key + jnp.arange(span_len, dtype=jnp.int32),
                (seq_dev, span_len),
            )
            return absorb(
                running, span_keys, span_values, key_pos, jnp.ones((seq_dev, span_len), bool)
            )

        return lax.fori_loop(0, row_count // span_len, one_span, state_now)

    row_max, row_sum, weighted = fold_piece(
        initial,
        (
            lax.all_gather(key_rows, "kv", axis=1, tiled=True),
            lax.all_gather(value_rows, "kv", axis=1, tiled=True),
        ),
        jnp.int32(0),
    )
    attended = (weighted / row_sum[..., None]).transpose(0, 3, 4, 1, 2, 5)
    attended = attended.reshape(seq_dev * tok_dev, heads_here * HD).astype(jnp.bfloat16)
    log_total = (row_max + jnp.log(row_sum)).reshape(seq_dev, heads_here, tok_dev)
    own_rows = model_width // n_tp

    def project():
        out_cols = lax.slice_in_dim(w_out, 0, own_rows * lax.axis_size("tp"), axis=1)
        return jnp.dot(attended, out_cols, preferred_element_type=jnp.float32).T

    scattered = lax.psum_scatter(
        project().astype(jnp.bfloat16), "tp", scatter_dimension=0, tiled=True
    ).astype(jnp.float32)
    mixed = scattered.T.reshape(seq_dev, tok_dev, own_rows).astype(jnp.bfloat16)
    return (mixed, log_total)


def solution(mesh):
    in_specs = (
        P("dp", "kv", "tp"),
        P(),
        P(None, "tp"),
        P(None, "tp"),
        P(None, "tp"),
        P(),
        P(),
        P("tp", None),
        P("dp", "kv", None),
    )
    out_specs = (P("dp", "kv", "tp"), P("dp", "tp", "kv"))
    return jax.shard_map(shards, mesh=mesh, in_specs=in_specs, out_specs=out_specs, check_vma=False)
```

profile of v0, /device:TPU:0, one launch (start us, length us, event | category | flops | bytes accessed | tf_op | source)
XLA Modules:
  0.0 81.3 jit_solution(10249953948225324526)
XLA Ops:
  7.2 0.0 copy-start
  7.2 0.0 copy-start.3
  7.2 0.0 copy-start.6
  7.2 0.0 copy-start.4
  7.2 0.0 reduce-scatter.2.cloned.1.call-start
  7.3 2.6 %all_gather.9 = bf16[1,256,1024]{2,1,0:T(8,128)(2,1)S(1)} all-gather(bf16[1,256,512]{2,1,0:T(8,128)(2,1)} %param.11), channel_id=1, replica_groups=mesh['dp'=4,'kv'=4,'tp'=2] {'tp'}, dimensions={2}, use_global_device_ids=true | all-gather | bytes 786432 | tf_op jit(solution)/shard_map/all_gather | solution.py:24
  9.9 0.2 fusion.20
  10.1 1.4 %convolution_convert_fusion.1 = bf16[256,128]{0,1:T(8,128)(2,1)S(1)} fusion(bf16[1024,128]{1,0:T(8,128)(2,1)} %param.15, bf16[1,256,1024]{2,1,0:T(8,128)(2,1)S(1)} %all_gather.9, f32[1024]{0:T(1024)} %param.12, f32[256]{0:T(256)S(1)} %add_rsqrt_fusion.2), kind=kOutput, calls=%fused_computation.39 | convolution fusion | flops 68190208 | bytes 857088 | tf_op jit(solution)/shard_map/dot_general | solution.py:53
  11.5 0.4 fusion.30
  12.0 0.1 multiply_convert_fusion
  12.0 16.2 %all_gather.10 = bf16[1,1024,2,64]{1,3,2,0:T(8,128)(2,1)} all-gather(bf16[1,256,2,64]{1,3,2,0:T(8,128)(2,1)S(1)} %multiply_convert_fusion), channel_id=1, replica_groups=mesh['dp'=4,'kv'=4,'tp'=2] {'kv'}, dimensions={1}, use_global_device_ids=true | all-gather | bytes 327680 | tf_op jit(solution)/shard_map/all_gather | solution.py:125
  28.2 14.6 %all_gather.11 = bf16[1,1024,2,64]{1,3,2,0:T(8,128)(2,1)S(1)} all-gather(bf16[1,256,2,64]{1,3,2,0:T(8,128)(2,1)S(1)} %bitcast.99), channel_id=1, replica_groups=mesh['dp'=4,'kv'=4,'tp'=2] {'kv'}, dimensions={1}, use_global_device_ids=true | all-gather | bytes 327680 | tf_op jit(solution)/shard_map/all_gather | solution.py:126
  42.8 1.3 %fusion.33 = (f32[256,512]{1,0:T(8,128)S(1)}, f32[256,512]{1,0:T(8,128)}) fusion(bf16[1024,512]{1,0:T(8,128)(2,1)S(1)} %copy-done, bf16[1,256,1024]{2,1,0:T(8,128)(2,1)S(1)} %all_gather.9, f32[1024]{0:T(1024)S(1)} %copy-done.3, f32[256]{0:T(256)S(1)} %add_rsqrt_fusion.2), kind=kOutput, calls=%fused_computation.59 | convolution fusion | flops 269615104 | bytes 2626560 | tf_op jit(solution)/shard_map/dot_general | solution.py:41
  44.1 0.2 copy.26
  44.3 0.0 copy-start.2
  44.4 0.1 rsqrt.30
  44.5 1.6 %reshape.336 = f32[1,8,32,2,4,64]{5,4,3,2,1,0:T(4,128)S(1)} reshape(f32[256,512]{1,0:T(8,128)} %get-tuple-element.319) | data formatting | bytes 1048576 | tf_op jit(solution)/shard_map/reshape | solution.py:41
  46.1 1.1 %fusion.24 = bf16[1,8,32,2,4,64]{5,2,4,1,3,0:T(8,128)(2,1)} fusion(f32[1,8,32,2,4,64]{5,4,3,2,1,0:T(4,128)S(1)} %reshape.336, f32[64]{0:T(128)S(1)} %copy-done.5, f32[8,32,2,4]{1,3,0,2:T(4,128)S(1)} %copy.27), kind=kLoop, calls=%fused_computation.45 | loop fusion | flops 393216 | bytes 794880 | tf_op jit(solution)/shard_map/convert_element_type | solution.py:45
  47.2 15.7 %while.20 = (s32[]{:T(128)}, f32[1,2,4,8,32]{4,2,3,1,0:T(4,128)S(1)}, f32[1,2,4,8,32]{4,2,3,1,0:T(4,128)S(1)}, f32[1,2,4,8,32,64]{5,4,3,2,1,0:T(8,128)S(1)}, s32...) while((s32[]{:T(128)}, ...), condition=%wide.region_7.8_spmd.clone, body=%wide.region_3.7_spmd.clone.sunk | while | flops 140261664 | bytes 9419611 | solution.py:120
  47.2 0.1 mul.331
  47.3 0.1 compare_reduce_fusion.2
  47.4 0.1 sub.166
  47.5 0.1 fusion.48
  47.7 0.1 subtract_convert_fusion.2
  47.8 1.7 %fusion.49 = (f32[2,4,8,32]{3,1,2,0:T(4,128)S(1)}, f32[1,2,4,8,32,256]{5,4,2,3,1,0:T(8,128)S(1)}) fusion(f32[8,32,256]{2,1,0:T(8,128)S(1)} %subtract_convert_fusion.2, f32[2,4]{1,0:T(2,128)S(1)} %mul.331, bf16[1,8,32,2,4,64]{5,2,4,1,3,0:T(8,128)(2,1)} %get-tuple-element.431, bf16[1,1024,2,64]{1,3,2,0:T(8,128)(2,1)} %get-tuple-element.430, ...), kind=kOutput, calls=%fused_computation.58.clone.1 | convolution fusion | flops 70252544 | bytes 3022884 | tf_op jit(solution)/shard_map/while/body/eval_jaxpr/sbqkgd,snkd->skgbqn/dot_general | solution.py:72
  49.6 0.8 %fusion.51 = (bf16[2,4,8,32,256]{4,3,1,2,0:T(8,128)(2,1)S(1)}, f32[2,4,8,32]{3,1,2,0:T(4,128)S(1)}) fusion(f32[1,2,4,8,32,256]{5,4,2,3,1,0:T(8,128)S(1)} %get-tuple-element.393, f32[2,4,8,32]{3,1,2,0:T(4,128)S(1)} %bitcast.92, pred[8,32,256]{2,1,0:T(8,128)(4,1)S(1)} %fusion.48), kind=kLoop, calls=%fused_computation.9.clone.1 | loop fusion | flops 2095104 | bytes 3227648 | tf_op jit(solution)/shard_map/reshape.263
  50.4 0.1 bitcast_add_fusion.2
  50.4 0.7 fusion.52
  51.2 0.1 mul.331
  51.3 0.1 compare_reduce_fusion.2
  51.4 0.1 sub.166
  51.5 0.1 fusion.48
  51.6 0.1 subtract_convert_fusion.2
  51.7 1.7 %fusion.49 = (f32[2,4,8,32]{3,1,2,0:T(4,128)S(1)}, f32[1,2,4,8,32,256]{5,4,2,3,1,0:T(8,128)S(1)}) fusion(f32[8,32,256]{2,1,0:T(8,128)S(1)} %subtract_convert_fusion.2, f32[2,4]{1,0:T(2,128)S(1)} %mul.331, bf16[1,8,32,2,4,64]{5,2,4,1,3,0:T(8,128)(2,1)} %get-tuple-element.431, bf16[1,1024,2,64]{1,3,2,0:T(8,128)(2,1)} %get-tuple-element.430, ...), kind=kOutput, calls=%fused_computation.58.clone.1 | convolution fusion | flops 70252544 | bytes 3022884 | tf_op jit(solution)/shard_map/while/body/eval_jaxpr/sbqkgd,snkd->skgbqn/dot_general | solution.py:72
  53.5 0.8 %fusion.51 = (bf16[2,4,8,32,256]{4,3,1,2,0:T(8,128)(2,1)S(1)}, f32[2,4,8,32]{3,1,2,0:T(4,128)S(1)}) fusion(f32[1,2,4,8,32,256]{5,4,2,3,1,0:T(8,128)S(1)} %get-tuple-element.393, f32[2,4,8,32]{3,1,2,0:T(4,128)S(1)} %bitcast.92, pred[8,32,256]{2,1,0:T(8,128)(4,1)S(1)} %fusion.48), kind=kLoop, calls=%fused_computation.9.clone.1 | loop fusion | flops 2095104 | bytes 3227648 | tf_op jit(solution)/shard_map/reshape.263
  54.3 0.1 bitcast_add_fusion.2
  54.4 0.6 fusion.52
  55.1 0.1 mul.331
  55.2 0.1 compare_reduce_fusion.2
  55.3 0.1 sub.166
  55.4 0.1 fusion.48
  55.5 0.1 subtract_convert_fusion.2
  55.6 1.7 %fusion.49 = (f32[2,4,8,32]{3,1,2,0:T(4,128)S(1)}, f32[1,2,4,8,32,256]{5,4,2,3,1,0:T(8,128)S(1)}) fusion(f32[8,32,256]{2,1,0:T(8,128)S(1)} %subtract_convert_fusion.2, f32[2,4]{1,0:T(2,128)S(1)} %mul.331, bf16[1,8,32,2,4,64]{5,2,4,1,3,0:T(8,128)(2,1)} %get-tuple-element.431, bf16[1,1024,2,64]{1,3,2,0:T(8,128)(2,1)} %get-tuple-element.430, ...), kind=kOutput, calls=%fused_computation.58.clone.1 | convolution fusion | flops 70252544 | bytes 3022884 | tf_op jit(solution)/shard_map/while/body/eval_jaxpr/sbqkgd,snkd->skgbqn/dot_general | solution.py:72
  57.4 0.8 %fusion.51 = (bf16[2,4,8,32,256]{4,3,1,2,0:T(8,128)(2,1)S(1)}, f32[2,4,8,32]{3,1,2,0:T(4,128)S(1)}) fusion(f32[1,2,4,8,32,256]{5,4,2,3,1,0:T(8,128)S(1)} %get-tuple-element.393, f32[2,4,8,32]{3,1,2,0:T(4,128)S(1)} %bitcast.92, pred[8,32,256]{2,1,0:T(8,128)(4,1)S(1)} %fusion.48), kind=kLoop, calls=%fused_computation.9.clone.1 | loop fusion | flops 2095104 | bytes 3227648 | tf_op jit(solution)/shard_map/reshape.263
  58.3 0.1 bitcast_add_fusion.2
  58.3 0.6 fusion.52
  59.0 0.1 mul.331
  59.1 0.1 compare_reduce_fusion.2
  59.2 0.1 sub.166
  59.3 0.1 fusion.48
  59.4 0.1 subtract_convert_fusion.2
  59.5 1.7 %fusion.49 = (f32[2,4,8,32]{3,1,2,0:T(4,128)S(1)}, f32[1,2,4,8,32,256]{5,4,2,3,1,0:T(8,128)S(1)}) fusion(f32[8,32,256]{2,1,0:T(8,128)S(1)} %subtract_convert_fusion.2, f32[2,4]{1,0:T(2,128)S(1)} %mul.331, bf16[1,8,32,2,4,64]{5,2,4,1,3,0:T(8,128)(2,1)} %get-tuple-element.431, bf16[1,1024,2,64]{1,3,2,0:T(8,128)(2,1)} %get-tuple-element.430, ...), kind=kOutput, calls=%fused_computation.58.clone.1 | convolution fusion | flops 70252544 | bytes 3022884 | tf_op jit(solution)/shard_map/while/body/eval_jaxpr/sbqkgd,snkd->skgbqn/dot_general | solution.py:72
  61.3 0.8 %fusion.51 = (bf16[2,4,8,32,256]{4,3,1,2,0:T(8,128)(2,1)S(1)}, f32[2,4,8,32]{3,1,2,0:T(4,128)S(1)}) fusion(f32[1,2,4,8,32,256]{5,4,2,3,1,0:T(8,128)S(1)} %get-tuple-element.393, f32[2,4,8,32]{3,1,2,0:T(4,128)S(1)} %bitcast.92, pred[8,32,256]{2,1,0:T(8,128)(4,1)S(1)} %fusion.48), kind=kLoop, calls=%fused_computation.9.clone.1 | loop fusion | flops 2095104 | bytes 3227648 | tf_op jit(solution)/shard_map/reshape.263
  62.2 0.1 bitcast_add_fusion.2
  62.2 0.7 fusion.52
  62.9 0.0 copy-start.1
  62.9 0.3 fusion.26
  63.3 0.4 copy.30
  63.7 0.3 convert_element_type.92
  64.0 0.1 copy-done.1
  64.1 1.2 %fusion.19 = bf16[1024,256]{0,1:T(8,128)(2,1)} fusion(bf16[256,512]{1,0:T(8,128)(2,1)S(1)} %convert_element_type.92, bf16[512,1024]{1,0:T(8,128)(2,1)S(1)} %copy-done.1), kind=kOutput, calls=%fused_computation.38 | convolution fusion | flops 268697600 | bytes 1835008 | tf_op jit(solution)/shard_map/dot_general | solution.py:137
  65.4 0.0 reduce-scatter.2.cloned.1.call-update
  65.4 0.7 reshape.338
  66.1 8.4 %reduce-scatter.2.cloned.1.call-done = bf16[512,256]{0,1:T(8,128)(2,1)} async-done(((bf16[1024,256]{0,1:T(8,128)(2,1)}), bf16[512,256]{0,1:T(8,128)(2,1)}) %reduce-scatter.2.cloned.1.call-update) | async-done | bytes 262160 | tf_op jit(solution)/shard_map/reduce_scatter | solution.py:139
  (43 shorter events, 0.4 us)
Async XLA Ops:
  7.2 35.7 %copy-start = (bf16[1024,512]{1,0:T(8,128)(2,1)S(1)}, bf16[1024,512]{1,0:T(8,128)(2,1)}, u32[]{:S(2)}) copy-start(bf16[1024,512]{1,0:T(8,128)(2,1)} %param.13) | copy-start | bytes 3145732
  7.2 4.3 %copy-start.3 = (f32[1024]{0:T(1024)S(1)}, f32[1024]{0:T(1024)}, u32[]{:S(2)}) copy-start(f32[1024]{0:T(1024)} %param.12) | copy-start | bytes 12292
  7.2 4.3 %copy-start.6 = (bf16[1024,128]{1,0:T(8,128)(2,1)S(1)}, bf16[1024,128]{1,0:T(8,128)(2,1)}, u32[]{:S(2)}) copy-start(bf16[1024,128]{1,0:T(8,128)(2,1)} %param.14) | copy-start | bytes 786436
  7.2 4.7 %copy-start.4 = (f32[64]{0:T(128)S(1)}, f32[64]{0:T(128)}, u32[]{:S(2)}) copy-start(f32[64]{0:T(128)} %param.17) | copy-start | bytes 772
  7.2 67.2 %reduce-scatter.2.cloned.1.call-start = ((), (), s32[]{:S(2)}) async-start(), calls=%async_computation.1 | async-start | bytes 786432 | tf_op jit(solution)/shard_map/reduce_scatter | solution.py:139
  44.1 2.0 %copy-start.5 = (f32[64]{0:T(128)S(1)}, f32[64]{0:T(128)}, u32[]{:S(2)}) copy-start(f32[64]{0:T(128)} %param.16) | copy-start | bytes 772
  44.3 2.9 %copy-start.2 = (s32[1,8,16]{2,1,0:T(8,128)S(1)}, s32[1,8,16]{2,1,0:T(8,128)}, u32[]{:S(2)}) copy-start(s32[1,8,16]{2,1,0:T(8,128)} %param.19) | copy-start | bytes 1540
  62.9 1.2 %copy-start.1 = (bf16[512,1024]{1,0:T(8,128)(2,1)S(1)}, bf16[512,1024]{1,0:T(8,128)(2,1)}, u32[]{:S(2)}) copy-start(bf16[512,1024]{1,0:T(8,128)(2,1)} %param.18) | copy-start | bytes 3145732
Sparse Core Ops, SparseCore 0:
  65.5 8.8 reduce-scatter.1
where the time goes:
time: 81.6 us; the launch traced here: 81.3 us
  blocking collectives  33.4 us (41%)
  between operations  14.3 us (18%)
  matrix products  13.8 us (17%)
  waiting for transfers between devices  8.37 us (10%)
  other arithmetic  6.92 us (8%)
  local copies, waits for them, and re-layouts  4.09 us (5%)
    all_gather x1, blocking collectives, shards(): lax.all_gather(key_rows, 'kv', axis=1, tiled=True)  16.2 us
    all_gather x1, blocking collectives, shards(): lax.all_gather(value_rows, 'kv', axis=1, tiled=True)  14.6 us
    reduce_scatter x1, waiting for transfers between devices, shards(): lax.psum_scatter(project().astype(jnp.bfloat16), 'tp', scatter_dimension=...  8.35 us
    dot_general x4, matrix products, absorb(): jnp.einsum('sbqkgd,snkd->skgbqn', queries, span_keys, preferred_element_t...  6.99 us
    another operation x4, other arithmetic  3.33 us
    all_gather x1, blocking collectives, shards(): gathered = lax.all_gather(tokens, 'tp', axis=2, tiled=True)  2.64 us
    dot_general x4, matrix products, absorb(): jnp.einsum('skgbqn,snkd->skgbqd', weights.astype(jnp.bfloat16), span_valu...  2.6 us
  transfers between devices with their start and end apart: 1, of which 1 were waited for; matrix products, arithmetic and copies ran while one was open for 1% of the time, Pallas kernels for 0%

commit v1 on v0

--- a/solution.py
+++ b/solution.py
@@ -122,7 +122,12 @@
     row_max, row_sum, weighted = fold_piece(
         initial,
         (
-            lax.all_gather(key_rows, "kv", axis=1, tiled=True),
+            jnp.concatenate(
+                jax.lax.all_to_all(
+                    jnp.stack([key_rows] * jax.lax.axis_size("kv"), axis=0), "kv", 0, 0
+                ),
+                axis=1,
+            ),
             lax.all_gather(value_rows, "kv", axis=1, tiled=True),
         ),
         jnp.int32(0),

time: 81.6 us -> 74.6 us (0.914)
  blocking collectives: 33.4 us -> 17.4 us
  starting transfers between devices: 0.04 us -> 6.23 us
  local copies, waits for them, and re-layouts: 4.09 us -> 5.78 us
    all_gather x1 -> x0, blocking collectives: 16.2 us -> none  [shards(): lax.all_gather(key_rows, 'kv', axis=1, tiled=True)]
    all_to_all x0 -> x1, starting transfers between devices: none -> 6.23 us  [shards(): jax.lax.all_to_all(jnp.stack([key_rows] * jax.lax.axis_size('kv'), axis=0...]
    dot_general x1, matrix products: 0.39 us -> 1.37 us  [shards(): jnp.dot(hidden, w_key, preferred_element_type=jnp.float32)]
    reshape x0 -> x1, local copies, waits for them, and re-layouts: none -> 0.97 us  [shards(): jnp.concatenate(jax.lax.all_to_all(jnp.stack([key_rows] * jax.lax.axis_si...]
  transfers between devices with their start and end apart: 1 -> 2, of which waited for: 1 -> 1; matrix products, arithmetic and copies ran while one was open for 1% -> 8% of each run, Pallas kernels for 0% -> 0%
where the time goes in v1:
time: 74.6 us; the launch traced here: 74 us
  blocking collectives  17.4 us (23%)
  matrix products  14.4 us (19%)
  between operations  14.2 us (19%)
  waiting for transfers between devices  8.76 us (12%)
  other arithmetic  6.89 us (9%)
  starting transfers between devices  6.23 us (8%)
  local copies, waits for them, and re-layouts  5.78 us (8%)
    all_gather x1, blocking collectives, shards(): lax.all_gather(value_rows, 'kv', axis=1, tiled=True)  14.8 us
    reduce_scatter x1, waiting for transfers between devices, shards(): lax.psum_scatter(project().astype(jnp.bfloat16), 'tp', scatter_dimension=...  8.74 us
    dot_general x4, matrix products, absorb(): jnp.einsum('sbqkgd,snkd->skgbqn', queries, span_keys, preferred_element_t...  6.88 us
    all_to_all x1, starting transfers between devices, shards(): jax.lax.all_to_all(jnp.stack([key_rows] * jax.lax.axis_size('kv'), axis=0...  6.23 us
    another operation x4, other arithmetic  3.31 us
    all_gather x1, blocking collectives, shards(): gathered = lax.all_gather(tokens, 'tp', axis=2, tiled=True)  2.64 us
    dot_general x4, matrix products, absorb(): jnp.einsum('skgbqn,snkd->skgbqd', weights.astype(jnp.bfloat16), span_valu...  2.57 us
    reshape x1, local copies, waits for them, and re-layouts, shards(): jnp.dot(hidden, w_query, preferred_element_type=jnp.float32)  1.59 us
  transfers between devices with their start and end apart: 2, of which 1 were waited for; matrix products, arithmetic and copies ran while one was open for 8% of the time, Pallas kernels for 0%

profile of v1, /device:TPU:0, one launch (start us, length us, event | category | flops | bytes accessed | tf_op | source)
XLA Modules:
  0.0 74.0 jit_solution(16567696017399093974)
XLA Ops:
  7.2 0.0 copy-start
  7.2 0.0 copy-start.3
  7.2 2.6 %all_gather.6 = bf16[1,256,1024]{2,1,0:T(8,128)(2,1)S(1)} all-gather(bf16[1,256,512]{2,1,0:T(8,128)(2,1)} %param.11), channel_id=1, replica_groups=mesh['dp'=4,'kv'=4,'tp'=2] {'tp'}, dimensions={2}, use_global_device_ids=true | all-gather | bytes 786432 | tf_op jit(solution)/shard_map/all_gather | solution.py:24
  9.9 0.2 fusion.20
  10.0 1.4 %bitcast_reduce_fusion.1 = (f32[256,2]{0,1:T(2,128)S(1)}, f32[256,128]{0,1:T(8,128)S(1)}) fusion(bf16[1024,128]{1,0:T(8,128)(2,1)} %param.14, bf16[1,256,1024]{2,1,0:T(8,128)(2,1)S(1)} %all_gather.6, f32[1024]{0:T(1024)} %param.12, f32[256]{0:T(256)S(1)} %add_rsqrt_fusion.2), kind=kOutput, calls=%fused_computation.50 | convolution fusion | flops 68222464 | bytes 924672 | tf_op jit(solution)/shard_map/dot_general | solution.py:47
  11.4 0.1 multiply_convert_fusion
  11.5 0.7 stack.2
  12.3 6.2 %all-to-all-start = ((bf16[4,1,256,2,64]{2,4,3,1,0:T(8,128)(2,1)}), bf16[4,1,256,2,64]{2,4,3,1,0:T(8,128)(2,1)}, u32[]{:S(2)}, u32[]{:S(2)}) async-start(bf16[4,1,256,2,64]{2,4,3,1,0:T(8,128)(2,1)} %stack.2), calls=%async_computation | async-start | bytes 524288 | tf_op jit(solution)/shard_map/all_to_all | solution.py:126
  18.5 1.0 %convolution_convert_fusion.1 = bf16[256,128]{0,1:T(8,128)(2,1)} fusion(bf16[1024,128]{1,0:T(8,128)(2,1)S(1)} %copy-done.6, bf16[1,256,1024]{2,1,0:T(8,128)(2,1)S(1)} %all_gather.6, f32[1024]{0:T(1024)S(1)} %copy-done.3, f32[256]{0:T(256)S(1)} %add_rsqrt_fusion.2), kind=kOutput, calls=%fused_computation.39 | convolution fusion | flops 68190208 | bytes 857088 | tf_op jit(solution)/shard_map/dot_general | solution.py:53
  19.5 1.3 %fusion.33 = (f32[256,512]{1,0:T(8,128)S(1)}, f32[256,512]{1,0:T(8,128)}) fusion(bf16[1024,512]{1,0:T(8,128)(2,1)S(1)} %copy-done, bf16[1,256,1024]{2,1,0:T(8,128)(2,1)S(1)} %all_gather.6, f32[1024]{0:T(1024)S(1)} %copy-done.3, f32[256]{0:T(256)S(1)} %add_rsqrt_fusion.2), kind=kOutput, calls=%fused_computation.59 | convolution fusion | flops 269615104 | bytes 2626560 | tf_op jit(solution)/shard_map/dot_general | solution.py:41
  20.8 0.2 copy.44
  21.0 0.0 copy-start.2
  21.1 0.1 rsqrt.30
  21.2 1.6 %reshape.337 = f32[1,8,32,2,4,64]{5,4,3,2,1,0:T(4,128)S(1)} reshape(f32[256,512]{1,0:T(8,128)} %get-tuple-element.321) | data formatting | bytes 1048576 | tf_op jit(solution)/shard_map/reshape | solution.py:41
  22.8 14.8 %all_gather.7 = bf16[1,1024,2,64]{1,3,2,0:T(8,128)(2,1)S(1)} all-gather(bf16[1,256,2,64]{1,3,2,0:T(8,128)(2,1)} %bitcast.105), channel_id=1, replica_groups=mesh['dp'=4,'kv'=4,'tp'=2] {'kv'}, dimensions={1}, use_global_device_ids=true | all-gather | bytes 327680 | tf_op jit(solution)/shard_map/all_gather | solution.py:131
  37.6 1.1 %fusion.24 = bf16[1,8,32,2,4,64]{5,2,4,1,3,0:T(8,128)(2,1)} fusion(f32[1,8,32,2,4,64]{5,4,3,2,1,0:T(4,128)S(1)} %reshape.337, f32[64]{0:T(128)S(1)} %copy-done.5, f32[8,32,2,4]{1,3,0,2:T(4,128)S(1)} %copy.45), kind=kLoop, calls=%fused_computation.45 | loop fusion | flops 393216 | bytes 794880 | tf_op jit(solution)/shard_map/convert_element_type | solution.py:45
  38.7 0.0 all-to-all-done
  38.7 1.0 %copy.52 = bf16[4,1,2,8,8,256]{5,4,0,3,2,1:T(8,128)(2,1)S(1)} copy(bf16[4,1,2,8,8,256]{5,4,3,2,1,0:T(8,128)(2,1)} %bitcast.32) | data formatting | bytes 524288 | tf_op jit(solution)/shard_map/reshape | solution.py:125
  39.7 15.5 %while.20 = (s32[]{:T(128)}, f32[1,2,4,8,32]{4,2,3,1,0:T(4,128)S(1)}, f32[1,2,4,8,32]{4,2,3,1,0:T(4,128)S(1)}, f32[1,2,4,8,32,64]{5,4,3,2,1,0:T(8,128)S(1)}, s32...) while((s32[]{:T(128)}, ...), condition=%wide.region_7.8_spmd.clone, body=%wide.region_3.7_spmd.clone.sunk | while | flops 140261664 | bytes 9158459 | solution.py:120
  39.7 0.1 mul.341
  39.8 0.1 compare_reduce_fusion.2
  39.9 0.1 sub.166
  40.0 0.1 fusion.48
  40.1 0.1 subtract_convert_fusion.2
  40.2 1.7 %fusion.49 = (f32[2,4,8,32]{3,1,2,0:T(4,128)S(1)}, f32[1,2,4,8,32,256]{5,4,2,3,1,0:T(8,128)S(1)}) fusion(f32[8,32,256]{2,1,0:T(8,128)S(1)} %subtract_convert_fusion.2, f32[2,4]{1,0:T(2,128)S(1)} %mul.341, bf16[1,8,32,2,4,64]{5,2,4,1,3,0:T(8,128)(2,1)} %get-tuple-element.433, bf16[1,1024,2,64]{1,3,2,0:T(8,128)(2,1)S(1)} %get-tuple-element.432, ...), kind=kOutput, calls=%fused_computation.58.clone.1 | convolution fusion | flops 70252544 | bytes 2761732 | tf_op jit(solution)/shard_map/while/body/eval_jaxpr/sbqkgd,snkd->skgbqn/dot_general | solution.py:72
  42.0 0.8 %fusion.51 = (bf16[2,4,8,32,256]{4,3,1,2,0:T(8,128)(2,1)S(1)}, f32[2,4,8,32]{3,1,2,0:T(4,128)S(1)}) fusion(f32[1,2,4,8,32,256]{5,4,2,3,1,0:T(8,128)S(1)} %get-tuple-element.395, f32[2,4,8,32]{3,1,2,0:T(4,128)S(1)} %bitcast.97, pred[8,32,256]{2,1,0:T(8,128)(4,1)S(1)} %fusion.48), kind=kLoop, calls=%fused_computation.9.clone.1 | loop fusion | flops 2095104 | bytes 3227648 | tf_op jit(solution)/shard_map/reshape.269
  42.8 0.1 bitcast_add_fusion.2
  42.9 0.7 fusion.52
  43.6 0.1 mul.341
  43.7 0.1 compare_reduce_fusion.2
  43.8 0.1 sub.166
  43.9 0.1 fusion.48
  44.0 0.1 subtract_convert_fusion.2
  44.1 1.7 %fusion.49 = (f32[2,4,8,32]{3,1,2,0:T(4,128)S(1)}, f32[1,2,4,8,32,256]{5,4,2,3,1,0:T(8,128)S(1)}) fusion(f32[8,32,256]{2,1,0:T(8,128)S(1)} %subtract_convert_fusion.2, f32[2,4]{1,0:T(2,128)S(1)} %mul.341, bf16[1,8,32,2,4,64]{5,2,4,1,3,0:T(8,128)(2,1)} %get-tuple-element.433, bf16[1,1024,2,64]{1,3,2,0:T(8,128)(2,1)S(1)} %get-tuple-element.432, ...), kind=kOutput, calls=%fused_computation.58.clone.1 | convolution fusion | flops 70252544 | bytes 2761732 | tf_op jit(solution)/shard_map/while/body/eval_jaxpr/sbqkgd,snkd->skgbqn/dot_general | solution.py:72
  45.9 0.8 %fusion.51 = (bf16[2,4,8,32,256]{4,3,1,2,0:T(8,128)(2,1)S(1)}, f32[2,4,8,32]{3,1,2,0:T(4,128)S(1)}) fusion(f32[1,2,4,8,32,256]{5,4,2,3,1,0:T(8,128)S(1)} %get-tuple-element.395, f32[2,4,8,32]{3,1,2,0:T(4,128)S(1)} %bitcast.97, pred[8,32,256]{2,1,0:T(8,128)(4,1)S(1)} %fusion.48), kind=kLoop, calls=%fused_computation.9.clone.1 | loop fusion | flops 2095104 | bytes 3227648 | tf_op jit(solution)/shard_map/reshape.269
  46.7 0.1 bitcast_add_fusion.2
  46.8 0.7 fusion.52
  47.5 0.1 mul.341
  47.6 0.1 compare_reduce_fusion.2
  47.7 0.1 sub.166
  47.8 0.1 fusion.48
  47.9 0.1 subtract_convert_fusion.2
  48.0 1.7 %fusion.49 = (f32[2,4,8,32]{3,1,2,0:T(4,128)S(1)}, f32[1,2,4,8,32,256]{5,4,2,3,1,0:T(8,128)S(1)}) fusion(f32[8,32,256]{2,1,0:T(8,128)S(1)} %subtract_convert_fusion.2, f32[2,4]{1,0:T(2,128)S(1)} %mul.341, bf16[1,8,32,2,4,64]{5,2,4,1,3,0:T(8,128)(2,1)} %get-tuple-element.433, bf16[1,1024,2,64]{1,3,2,0:T(8,128)(2,1)S(1)} %get-tuple-element.432, ...), kind=kOutput, calls=%fused_computation.58.clone.1 | convolution fusion | flops 70252544 | bytes 2761732 | tf_op jit(solution)/shard_map/while/body/eval_jaxpr/sbqkgd,snkd->skgbqn/dot_general | solution.py:72
  49.8 0.8 %fusion.51 = (bf16[2,4,8,32,256]{4,3,1,2,0:T(8,128)(2,1)S(1)}, f32[2,4,8,32]{3,1,2,0:T(4,128)S(1)}) fusion(f32[1,2,4,8,32,256]{5,4,2,3,1,0:T(8,128)S(1)} %get-tuple-element.395, f32[2,4,8,32]{3,1,2,0:T(4,128)S(1)} %bitcast.97, pred[8,32,256]{2,1,0:T(8,128)(4,1)S(1)} %fusion.48), kind=kLoop, calls=%fused_computation.9.clone.1 | loop fusion | flops 2095104 | bytes 3227648 | tf_op jit(solution)/shard_map/reshape.269
  50.7 0.1 bitcast_add_fusion.2
  50.7 0.6 fusion.52
  51.4 0.1 mul.341
  51.5 0.1 compare_reduce_fusion.2
  51.6 0.1 sub.166
  51.7 0.1 fusion.48
  51.8 0.1 subtract_convert_fusion.2
  51.9 1.7 %fusion.49 = (f32[2,4,8,32]{3,1,2,0:T(4,128)S(1)}, f32[1,2,4,8,32,256]{5,4,2,3,1,0:T(8,128)S(1)}) fusion(f32[8,32,256]{2,1,0:T(8,128)S(1)} %subtract_convert_fusion.2, f32[2,4]{1,0:T(2,128)S(1)} %mul.341, bf16[1,8,32,2,4,64]{5,2,4,1,3,0:T(8,128)(2,1)} %get-tuple-element.433, bf16[1,1024,2,64]{1,3,2,0:T(8,128)(2,1)S(1)} %get-tuple-element.432, ...), kind=kOutput, calls=%fused_computation.58.clone.1 | convolution fusion | flops 70252544 | bytes 2761732 | tf_op jit(solution)/shard_map/while/body/eval_jaxpr/sbqkgd,snkd->skgbqn/dot_general | solution.py:72
  53.7 0.8 %fusion.51 = (bf16[2,4,8,32,256]{4,3,1,2,0:T(8,128)(2,1)S(1)}, f32[2,4,8,32]{3,1,2,0:T(4,128)S(1)}) fusion(f32[1,2,4,8,32,256]{5,4,2,3,1,0:T(8,128)S(1)} %get-tuple-element.395, f32[2,4,8,32]{3,1,2,0:T(4,128)S(1)} %bitcast.97, pred[8,32,256]{2,1,0:T(8,128)(4,1)S(1)} %fusion.48), kind=kLoop, calls=%fused_computation.9.clone.1 | loop fusion | flops 2095104 | bytes 3227648 | tf_op jit(solution)/shard_map/reshape.269
  54.5 0.1 bitcast_add_fusion.2
  54.6 0.6 fusion.52
  55.2 0.0 copy-start.1
  55.3 0.3 fusion.26
  55.6 0.4 copy.48
  56.0 0.3 convert_element_type.91
  56.4 0.1 copy-done.1
  56.5 1.3 %fusion.19 = bf16[1024,256]{0,1:T(8,128)(2,1)} fusion(bf16[256,512]{1,0:T(8,128)(2,1)S(1)} %convert_element_type.91, bf16[512,1024]{1,0:T(8,128)(2,1)S(1)} %copy-done.1), kind=kOutput, calls=%fused_computation.38 | convolution fusion | flops 268697600 | bytes 1835008 | tf_op jit(solution)/shard_map/dot_general | solution.py:142
  57.7 0.0 reduce-scatter.2.cloned.1.call-update
  57.8 0.7 reshape.339
  58.4 8.7 %reduce-scatter.2.cloned.1.call-done = bf16[512,256]{0,1:T(8,128)(2,1)} async-done(((bf16[1024,256]{0,1:T(8,128)(2,1)}), bf16[512,256]{0,1:T(8,128)(2,1)}) %reduce-scatter.2.cloned.1.call-update) | async-done | bytes 262160 | tf_op jit(solution)/shard_map/reduce_scatter | solution.py:144
  (45 shorter events, 0.4 us)
Async XLA Ops:
  7.2 12.3 %copy-start = (bf16[1024,512]{1,0:T(8,128)(2,1)S(1)}, bf16[1024,512]{1,0:T(8,128)(2,1)}, u32[]{:S(2)}) copy-start(bf16[1024,512]{1,0:T(8,128)(2,1)} %param.13) | copy-start | bytes 3145732
  7.2 11.3 %copy-start.3 = (f32[1024]{0:T(1024)S(1)}, f32[1024]{0:T(1024)}, u32[]{:S(2)}) copy-start(f32[1024]{0:T(1024)} %param.12) | copy-start | bytes 12292
  7.2 4.2 %copy-start.4 = (f32[64]{0:T(128)S(1)}, f32[64]{0:T(128)}, u32[]{:S(2)}) copy-start(f32[64]{0:T(128)} %param.17) | copy-start | bytes 772
  7.2 11.3 %copy-start.6 = (bf16[1024,128]{1,0:T(8,128)(2,1)S(1)}, bf16[1024,128]{1,0:T(8,128)(2,1)}, u32[]{:S(2)}) copy-start(bf16[1024,128]{1,0:T(8,128)(2,1)} %param.15) | copy-start | bytes 786436
  12.3 26.4 %all-to-all-start = ((bf16[4,1,256,2,64]{2,4,3,1,0:T(8,128)(2,1)}), bf16[4,1,256,2,64]{2,4,3,1,0:T(8,128)(2,1)}, u32[]{:S(2)}, u32[]{:S(2)}) async-start(bf16[4,1,256,2,64]{2,4,3,1,0:T(8,128)(2,1)} %stack.2), calls=%async_computation | async-start | bytes 524288 | tf_op jit(solution)/shard_map/all_to_all | solution.py:126
  18.5 48.7 %reduce-scatter.2.cloned.1.call-start = ((), (), s32[]{:S(2)}) async-start(), calls=%async_computation.2 | async-start | bytes 786432 | tf_op jit(solution)/shard_map/reduce_scatter | solution.py:144
  20.8 16.8 %copy-start.5 = (f32[64]{0:T(128)S(1)}, f32[64]{0:T(128)}, u32[]{:S(2)}) copy-start(f32[64]{0:T(128)} %param.16) | copy-start | bytes 772
  21.0 18.6 %copy-start.2 = (s32[1,8,16]{2,1,0:T(8,128)S(1)}, s32[1,8,16]{2,1,0:T(8,128)}, u32[]{:S(2)}) copy-start(s32[1,8,16]{2,1,0:T(8,128)} %param.19) | copy-start | bytes 1540
  55.2 1.2 %copy-start.1 = (bf16[512,1024]{1,0:T(8,128)(2,1)S(1)}, bf16[512,1024]{1,0:T(8,128)(2,1)}, u32[]{:S(2)}) copy-start(bf16[512,1024]{1,0:T(8,128)(2,1)} %param.18) | copy-start | bytes 3145732
Sparse Core Ops, SparseCore 0:
  57.9 9.2 reduce-scatter.1
